TPU v7x, 256 devices: a whole 4x4x8 slice. The times are simulated.
256 devices in a mesh: ep: 16 (over y, x), tp: 16 (over z, core).
Axes of the slice: x: 4, y: 4, z: 8, core: 2. Of those that a mesh axis runs over, the one named last changes fastest.
Arguments:
- mix_tokens: bfloat16 [16384, 1, 1024], P(('ep', 'tp')), may hold values from -6 to 6
- mix_gain: float32 [1024], replicated, may hold values from 0.1 to 1.9
- w_query: bfloat16 [1024, 1024], replicated, may hold values from -0.1875 to 0.1875
- w_key: bfloat16 [1024, 256], replicated, may hold values from -0.1875 to 0.1875
- w_value: bfloat16 [1024, 256], replicated, may hold values from -0.1875 to 0.1875
- query_gain: float32 [64], replicated, may hold values from 1.2 to 14
- key_gain: float32 [64], replicated, may hold values from 1.2 to 14
- w_out: bfloat16 [1024, 1024], replicated, may hold values from -0.1875 to 0.1875
- expert_tokens: bfloat16 [32768, 1024], P(('ep', 'tp')), may hold values from -6 to 6
- expert_gain: float32 [1024], replicated, may hold values from 0.1 to 1.9
- route_ids: int32 [32768, 2], P(('ep', 'tp')), may hold values from 0 to 31, all different within a row; in each aligned block of 128 rows (0 to 127, 128 to 255, ...) at most 9 rows name the same one
- route_weights: float32 [32768, 2], P(('ep', 'tp')), may hold values from 0.1 to 1
- w_gate: bfloat16 [32, 1024, 4096], P('ep', None, 'tp'), may hold values from -0.1875 to 0.1875
- w_up: bfloat16 [32, 1024, 4096], P('ep', None, 'tp'), may hold values from -0.1875 to 0.1875
- w_down: bfloat16 [32, 4096, 1024], P('ep', 'tp'), may hold values from -0.09375 to 0.09375
Outputs:
- mix_out: bfloat16 [16384, 1, 1024], P(('ep', 'tp'))
- experts_out: bfloat16 [32768, 1024], P(('ep', 'tp'))
Inputs may be any that keep to these rules, and one draw needn't show every extreme that they name: `route_ids`: each row names 2 different experts. Among the rows of one device no expert is named more than 9 times, and in every draw some expert is named exactly 9 times by the rows of some device.
All inputs are finite; a program needn't handle non-finite values.
Results may differ from a plain program's by a relative error of at most 0.018.
The roundings to bfloat16 on the way count: a program that leaves them out, or rounds other values in their place, can miss the bound.
Values may be sent and summed in bfloat16 or wider, within the bound.
A program may use at most 128 MiB of HBM per device.

v0:
```python
import math
import jax
import jax.numpy as jnp
from jax import lax
from jax.sharding import PartitionSpec as P

HEAD = 64
GRID_W = 64
epsilon = 1e-06


def normalize(values, gain_vec):
    widened = values.astype(jnp.float32)
    return (
        widened
        * lax.rsqrt(jnp.mean(widened * widened, axis=-1, keepdims=True) + epsilon)
        * gain_vec
    )


def angle_tables(positions, head_size):
    quarter = head_size // 4
    frequency = 10000.0 ** (-jnp.arange(quarter, dtype=jnp.float32) / quarter)
    grid_pos = jnp.stack([positions // GRID_W, positions % GRID_W], axis=-1).astype(jnp.float32)
    angles = grid_pos[:, :, None] * frequency[None, None, :]
    return (jnp.cos(angles), jnp.sin(angles))


def turn(values, cosine_table, sine_table):
    shaped = values.shape
    quarter = shaped[-1] // 4
    leading = (shaped[0],) + (1,) * (len(shaped) - 2) + (2, quarter)
    cosine_table = cosine_table.reshape(leading)
    sine_table = sine_table.reshape(leading)
    halves = values.reshape(shaped[:-1] + (2, 2, quarter))
    first_part = halves[..., 0, :]
    second_part = halves[..., 1, :]
    turned = jnp.stack(
        [
            first_part * cosine_table - second_part * sine_table,
            first_part * sine_table + second_part * cosine_table,
        ],
        axis=-2,
    )
    return turned.reshape(shaped)


def attend(queries, fold_state, key_piece):
    key_rows = key_piece.shape[0]
    block_rows = math.gcd(key_rows, 1024)
    blocks = key_piece.reshape((key_rows // block_rows, block_rows) + key_piece.shape[1:])
    score_scale = HEAD ** (-0.5)

    def step_block(carried, block_keys):
        running_max, totals, accumulated = carried
        keys_part = block_keys[..., :HEAD]
        values_part = block_keys[..., HEAD:]
        scores = (
            jnp.einsum("qshd,ksd->qshk", queries, keys_part, preferred_element_type=jnp.float32)
            * score_scale
        )
        new_max = jnp.maximum(running_max, jnp.max(scores, axis=-1))
        shrink = jnp.exp(running_max - new_max)
        raised = jnp.exp(scores - new_max[..., None])
        totals = totals * shrink + jnp.sum(raised, axis=-1)
        accumulated = accumulated * shrink[..., None] + jnp.einsum(
            "qshk,ksd->qshd",
            raised.astype(jnp.bfloat16),
            values_part,
            preferred_element_type=jnp.float32,
        )
        return ((new_max, totals, accumulated), None)

    return lax.scan(step_block, fold_state, blocks)[0]


def mixer_half(mix_tokens, mix_gain, w_query, w_key, w_value, query_gain, key_gain, w_out):
    tp_count = lax.axis_size("tp")
    seq_rows, sequences, model_width = mix_tokens.shape
    head_count = w_query.shape[1] // HEAD
    key_heads = w_key.shape[1] // HEAD
    local_heads = head_count // tp_count
    normed = normalize(mix_tokens, mix_gain).astype(jnp.bfloat16)
    queries = jnp.dot(normed, w_query, preferred_element_type=jnp.float32).astype(jnp.bfloat16)
    keys_raw = jnp.dot(normed, w_key, preferred_element_type=jnp.float32).astype(jnp.bfloat16)
    values = jnp.dot(normed, w_value, preferred_element_type=jnp.float32).astype(jnp.bfloat16)
    queries = queries.reshape(seq_rows, sequences, tp_count, local_heads * HEAD)
    key_value = jnp.concatenate(
        [
            keys_raw.reshape(seq_rows, sequences, key_heads, HEAD),
            values.reshape(seq_rows, sequences, key_heads, HEAD),
        ],
        axis=-1,
    )
    key_value = jnp.repeat(key_value, tp_count // key_heads, axis=2)
    packed = jnp.concatenate([queries, key_value], axis=-1)
    arrived = lax.all_to_all(packed, "tp", split_axis=2, concat_axis=0, tiled=True)
    span_rows = arrived.shape[0]
    positions = lax.axis_index("ep") * span_rows + jnp.arange(span_rows, dtype=jnp.int32)
    cosine_table, sine_table = angle_tables(positions, HEAD)
    query_width = local_heads * HEAD
    own_queries = normalize(
        arrived[:, :, 0, :query_width].reshape(span_rows, sequences, local_heads, HEAD), query_gain
    )
    own_queries = turn(own_queries, cosine_table, sine_table).astype(jnp.bfloat16)
    own_keys = normalize(arrived[:, :, 0, query_width : query_width + HEAD], key_gain)
    own_keys = turn(own_keys, cosine_table, sine_table).astype(jnp.bfloat16)
    key_pairs = jnp.concatenate([own_keys, arrived[:, :, 0, query_width + HEAD :]], axis=-1)
    start_state = (
        jnp.full((span_rows, sequences, local_heads), -1e30, jnp.float32),
        jnp.zeros((span_rows, sequences, local_heads), jnp.float32),
        jnp.zeros((span_rows, sequences, local_heads, HEAD), jnp.float32),
    )
    running_max, totals, accumulated = attend(
        own_queries, start_state, lax.all_gather(key_pairs, "ep", axis=0, tiled=True)
    )
    mixed = (
        (accumulated / totals[..., None])
        .astype(jnp.bfloat16)
        .reshape(span_rows, sequences, query_width)
    )
    returned = lax.all_to_all(mixed, "tp", split_axis=0, concat_axis=2, tiled=True)
    return jnp.dot(returned, w_out, preferred_element_type=jnp.float32).astype(jnp.bfloat16)


def joint_hidden(w_gate, w_up, piece_rows):
    gate_act = jnp.einsum("rjd,jdf->rjf", piece_rows, w_gate, preferred_element_type=jnp.float32)
    up_act = jnp.einsum("rjd,jdf->rjf", piece_rows, w_up, preferred_element_type=jnp.float32)
    return (jax.nn.silu(gate_act) * up_act).astype(jnp.bfloat16)


def joint_down(hidden_all, w_down):
    group_sum = jnp.einsum(
        "rjf,jfd->rjd", hidden_all, w_down, preferred_element_type=jnp.float32
    ).astype(jnp.bfloat16)
    return lax.optimization_barrier(group_sum).astype(jnp.float32)


def expert_half(expert_tokens, expert_gain, route_ids, route_weights, w_gate, w_up, w_down):
    ep_count = lax.axis_size("ep")
    tok_count, model_width = expert_tokens.shape
    top_count = route_ids.shape[1]
    local_experts = w_gate.shape[0]
    expert_count = local_experts * ep_count
    capacity = tok_count * top_count * 9 // (8 * expert_count)
    slot_count = ep_count * capacity * local_experts
    normed = normalize(expert_tokens, expert_gain).astype(jnp.bfloat16)
    flat_ids = route_ids.reshape(-1)
    matches = (flat_ids[:, None] == jnp.arange(expert_count, dtype=jnp.int32)[None, :]).astype(
        jnp.int32
    )
    rank_ids = jnp.sum((jnp.cumsum(matches, axis=0) - 1) * matches, axis=1)
    slot_ids = (
        flat_ids // local_experts * capacity + rank_ids
    ) * local_experts + flat_ids % local_experts
    chosen = slot_ids.reshape(tok_count, top_count)
    dispatch = jnp.sum(
        (chosen[:, :, None] == jnp.arange(slot_count, dtype=jnp.int32)[None, None, :]).astype(
            jnp.bfloat16
        ),
        axis=1,
    )
    outgoing = lax.dot_general(
        dispatch, normed, (((0,), (0,)), ((), ())), preferred_element_type=jnp.float32
    )
    outgoing = outgoing.astype(jnp.bfloat16).reshape(ep_count, capacity, local_experts, model_width)
    incoming = lax.all_to_all(outgoing, "ep", split_axis=0, concat_axis=0, tiled=True)
    own_rows = ep_count * capacity
    incoming = incoming.reshape(own_rows, local_experts, model_width)
    hidden_all = joint_hidden(w_gate, w_up, lax.all_gather(incoming, "tp", axis=0, tiled=True))
    summed = lax.psum_scatter(
        joint_down(hidden_all, w_down).astype(jnp.bfloat16), "tp", scatter_dimension=0, tiled=True
    )
    expert_results = summed.reshape(ep_count, capacity, local_experts, model_width)
    returned = lax.all_to_all(
        expert_results, "ep", split_axis=0, concat_axis=0, tiled=True
    ).reshape(slot_count, model_width)
    picked = jnp.take(returned, slot_ids, axis=0).reshape(tok_count, top_count, model_width)
    combined = jnp.sum(route_weights[:, :, None] * picked.astype(jnp.float32), axis=1)
    return combined.astype(jnp.bfloat16)


def body(
    mix_tokens,
    mix_gain,
    w_query,
    w_key,
    w_value,
    query_gain,
    key_gain,
    w_out,
    expert_tokens,
    expert_gain,
    route_ids,
    route_weights,
    w_gate,
    w_up,
    w_down,
):
    mix_out = mixer_half(mix_tokens, mix_gain, w_query, w_key, w_value, query_gain, key_gain, w_out)
    experts_out = expert_half(
        expert_tokens, expert_gain, route_ids, route_weights, w_gate, w_up, w_down
    )
    return (mix_out, experts_out)


def solution(mesh):
    placed = (
        P(("ep", "tp"), None, None),
        P(),
        P(),
        P(),
        P(),
        P(),
        P(),
        P(),
        P(("ep", "tp"), None),
        P(),
        P(("ep", "tp"), None),
        P(("ep", "tp"), None),
        P("ep", None, "tp"),
        P("ep", None, "tp"),
        P("ep", "tp", None),
    )
    return jax.shard_map(
        body,
        mesh=mesh,
        in_specs=placed,
        out_specs=(P(("ep", "tp"), None, None), P(("ep", "tp"), None)),
        check_vma=False,
    )
```

profile of v0, /device:TPU:1, one launch (start us, length us, event | category | flops | bytes accessed | tf_op | source)
XLA Modules:
  0.0 339.7 jit_solution(8806245419591874709)
XLA Ops:
  13.0 18.7 %all_to_all.43 = bf16[16,9,2,1024]{3,2,1,0:T(2,128)(2,1)S(1)} all-to-all(bf16[16,9,2,1024]{3,2,1,0:T(2,128)(2,1)S(1)} %reshape.571), channel_id=1, replica_groups=mesh['ep'=16,'tp'=16] {'ep'}, dimensions={0} | all-to-all | bytes 1179648 | tf_op jit(solution)/shard_map/all_to_all | solution.py:167
  37.7 10.4 %all-to-all-start = ((bf16[64,1,16,192]{3,0,1,2:T(8,128)(2,1)}), bf16[64,1,16,192]{3,0,1,2:T(8,128)(2,1)S(1)}, u32[]{:S(2)}, u32[]{:S(2)}) async-start(bf16[64,1,16,192]{3,0,1,2:T(8,128)(2,1)} %pad_maximum_fusion), calls=%async_computation | async-start | bytes 1048576 | tf_op jit(solution)/shard_map/all_to_all | solution.py:97
  48.3 22.1 %all-to-all-done = bf16[64,1,16,192]{3,0,1,2:T(8,128)(2,1)S(1)} async-done(((bf16[64,1,16,192]{3,0,1,2:T(8,128)(2,1)}), bf16[64,1,16,192]{3,0,1,2:T(8,128)(2,1)S(1)}, u32[]{:S(2)}, u32[]{:S(2)}) %all-to-all-start) | async-done | bytes 393248 | tf_op jit(solution)/shard_map/all_to_all | solution.py:97
  77.2 28.6 %all-gather.5.cloned.1.call-done = bf16[2304,2,1024]{2,0,1:T(8,128)(2,1)} async-done(((bf16[144,2,1024]{2,0,1:T(8,128)(2,1)}), bf16[2304,2,1024]{2,0,1:T(8,128)(2,1)}) %all-gather.5.cloned.1.call-update) | async-done | bytes 9437200 | tf_op jit(solution)/shard_map/all_gather | solution.py:170
  105.8 8.7 %convolution_bitcast_fusion.1 = f32[2304,2,256]{2,0,1:T(8,128)} fusion(bf16[2304,2,1024]{2,0,1:T(8,128)(2,1)} %all-gather.5.cloned.1.call-done, bf16[2,1024,256]{2,1,0:T(8,128)(2,1)} %param.29), kind=kOutput, calls=%fused_computation.26 | convolution fusion | flops 2415919104 | bytes 15204352 | tf_op jit(solution)/shard_map/rjd,jdf->rjf/dot_general | solution.py:127
  114.5 11.7 %convert_bitcast_fusion = bf16[2304,2,1024]{2,0,1:T(8,128)(2,1)} fusion(bf16[2,256,1024]{2,1,0:T(8,128)(2,1)} %param.31, bf16[2304,2,1024]{2,0,1:T(8,128)(2,1)} %all-gather.5.cloned.1.call-done, bf16[2,1024,256]{2,1,0:T(8,128)(2,1)} %param.30, f32[2304,2,256]{2,0,1:T(8,128)} %convolution_bitcast_fusion.1), kind=kOutput, calls=%fused_computation.23 | convolution fusion | flops 4843634688 | bytes 25690112 | tf_op jit(solution)/shard_map/rjf,jfd->rjd/dot_general | solution.py:133
  126.2 36.4 %all-gather.3.cloned.1.call-done = bf16[16384,1,128]{2,0,1:T(8,128)(2,1)} async-done(((bf16[1024,1,128]{2,0,1:T(8,128)(2,1)}), bf16[16384,1,128]{2,0,1:T(8,128)(2,1)}) %all-gather.3.cloned.1.call-update) | async-done | bytes 4194320 | tf_op jit(solution)/shard_map/all_gather | solution.py:115
  162.7 131.4 %while.15 = (s32[]{:T(128)}, f32[1024,1,1]{0,2,1:T(1,128)S(1)}, f32[1024,1,1]{0,2,1:T(1,128)S(1)}, f32[1024,1,1,64]{0,3,2,1:T(8,128)S(1)}, bf16[16,1024,1,128]{3...) while((s32[]{:T(128)}, f32[1024,1,1]{0,2,1:T(1,128)S(1)}, ...), condition=%wide.region_6.7_spmd.clone, body=%wide.region_3.6_spmd.clone.sunk | while | flops 277025792 | bytes 31129728 | solution.py:74
  166.4 3.1 fusion.81
  174.5 3.2 fusion.81
  183.0 3.2 fusion.81
  191.3 3.2 fusion.81
  199.6 3.2 fusion.81
  207.9 3.2 fusion.81
  216.2 3.2 fusion.81
  224.5 3.2 fusion.81
  232.8 3.2 fusion.81
  241.1 3.1 fusion.81
  249.2 3.1 fusion.81
  257.3 3.1 fusion.81
  296.4 7.9 %all-to-all-start.1 = ((bf16[16,2,2048]{2,1,0:T(2,128)(2,1)}), bf16[16,2,2048]{2,1,0:T(2,128)(2,1)S(1)}, u32[]{:S(2)}, u32[]{:S(2)}) async-start(bf16[16,2,2048]{2,1,0:T(2,128)(2,1)} %reshape.590), calls=%async_computation.1 | async-start | bytes 262144 | tf_op jit(solution)/shard_map/all_to_all | solution.py:122
  307.1 6.0 %all-to-all-done.1 = bf16[16,2,2048]{2,1,0:T(2,128)(2,1)S(1)} async-done(((bf16[16,2,2048]{2,1,0:T(2,128)(2,1)}), bf16[16,2,2048]{2,1,0:T(2,128)(2,1)S(1)}, u32[]{:S(2)}, u32[]{:S(2)}) %all-to-all-start.1) | async-done | bytes 131104 | tf_op jit(solution)/shard_map/all_to_all | solution.py:122
  313.1 4.2 %all-to-all-start.3 = ((bf16[16,9,2,1024]{3,2,1,0:T(2,128)(2,1)}), bf16[16,9,2,1024]{3,2,1,0:T(2,128)(2,1)S(1)}, u32[]{:S(2)}, u32[]{:S(2)}) async-start(bf16[16,9,2,1024]{3,2,1,0:T(2,128)(2,1)} %bitcast.24), calls=%async_computation.4 | async-start | bytes 1179648 | tf_op jit(solution)/shard_map/all_to_all | solution.py:175
  321.5 7.7 %all-to-all-done.3 = bf16[16,9,2,1024]{3,2,1,0:T(2,128)(2,1)S(1)} async-done(((bf16[16,9,2,1024]{3,2,1,0:T(2,128)(2,1)}), bf16[16,9,2,1024]{3,2,1,0:T(2,128)(2,1)S(1)}, u32[]{:S(2)}, u32[]{:S(2)}) %all-to-all-start.3) | async-done | bytes 589856 | tf_op jit(solution)/shard_map/all_to_all | solution.py:175
  (225 shorter events, 124.9 us)
Async XLA Ops:
  7.2 28.7 %copy-start = (bf16[1024,1024]{1,0:T(8,128)(2,1)S(1)}, bf16[1024,1024]{1,0:T(8,128)(2,1)}, u32[]{:S(2)}) copy-start(bf16[1024,1024]{1,0:T(8,128)(2,1)} %param.19) | copy-start | bytes 6291460
  7.2 25.5 %copy-start.2 = (bf16[64,1,1024]{2,0,1:T(8,128)(2,1)S(1)}, bf16[64,1,1024]{2,0,1:T(8,128)(2,1)}, u32[]{:S(2)}) copy-start(bf16[64,1,1024]{2,0,1:T(8,128)(2,1)} %param.17) | copy-start | bytes 393220
  7.2 25.7 %copy-start.3 = (f32[1024]{0:T(1024)S(1)}, f32[1024]{0:T(1024)}, u32[]{:S(2)}) copy-start(f32[1024]{0:T(1024)} %param.18) | copy-start | bytes 12292
  7.2 98.6 %all-gather.5.cloned.1.call-start = ((), (), s32[]{:S(2)}) async-start(), calls=%async_computation.6 | async-start | bytes 10027008 | tf_op jit(solution)/shard_map/all_gather | solution.py:170
  32.7 15.4 %copy-start.6 = (f32[64]{0:T(128)S(1)}, f32[64]{0:T(128)}, u32[]{:S(2)}) copy-start(f32[64]{0:T(128)} %param.23) | copy-start | bytes 772
  36.7 39.9 %copy-start.5 = (f32[64]{0:T(128)S(1)}, f32[64]{0:T(128)}, u32[]{:S(2)}) copy-start(f32[64]{0:T(128)} %param.22) | copy-start | bytes 772
  37.7 32.7 %all-to-all-start = ((bf16[64,1,16,192]{3,0,1,2:T(8,128)(2,1)}), bf16[64,1,16,192]{3,0,1,2:T(8,128)(2,1)S(1)}, u32[]{:S(2)}, u32[]{:S(2)}) async-start(bf16[64,1,16,192]{3,0,1,2:T(8,128)(2,1)} %pad_maximum_fusion), calls=%async_computation | async-start | bytes 1048576 | tf_op jit(solution)/shard_map/all_to_all | solution.py:97
  48.1 114.6 %all-gather.3.cloned.1.call-start = ((), (), s32[]{:S(2)}) async-start(), calls=%async_computation.5 | async-start | bytes 4456448 | tf_op jit(solution)/shard_map/all_gather | solution.py:115
  75.1 229.5 %reduce-scatter.2.cloned.1.call-start = ((), (), s32[]{:S(2)}) async-start(), calls=%async_computation.7 | async-start | bytes 10027008 | tf_op jit(solution)/shard_map/reduce_scatter | solution.py:171
  162.7 141.9 %copy-start.4 = (f32[128,2]{0,1:T(2,128)S(1)}, f32[128,2]{0,1:T(2,128)}, u32[]{:S(2)}) copy-start(f32[128,2]{0,1:T(2,128)} %param.28) | copy-start | bytes 3076
  174.5 3.9 %copy-start.1 = (f32[1024,1024]{1,0:T(8,128)S(1)}, f32[1024,1024]{1,0:T(8,128)}, u32[]{:S(2)}) copy-start(f32[1024,1024]{1,0:T(8,128)} %get-tuple-element.163) | copy-start | bytes 12582916 | tf_op jit(solution)/shard_map/while
  183.0 3.6 %copy-start.1 = (f32[1024,1024]{1,0:T(8,128)S(1)}, f32[1024,1024]{1,0:T(8,128)}, u32[]{:S(2)}) copy-start(f32[1024,1024]{1,0:T(8,128)} %get-tuple-element.163) | copy-start | bytes 12582916 | tf_op jit(solution)/shard_map/while
  191.3 3.6 %copy-start.1 = (f32[1024,1024]{1,0:T(8,128)S(1)}, f32[1024,1024]{1,0:T(8,128)}, u32[]{:S(2)}) copy-start(f32[1024,1024]{1,0:T(8,128)} %get-tuple-element.163) | copy-start | bytes 12582916 | tf_op jit(solution)/shard_map/while
  199.6 3.6 %copy-start.1 = (f32[1024,1024]{1,0:T(8,128)S(1)}, f32[1024,1024]{1,0:T(8,128)}, u32[]{:S(2)}) copy-start(f32[1024,1024]{1,0:T(8,128)} %get-tuple-element.163) | copy-start | bytes 12582916 | tf_op jit(solution)/shard_map/while
  207.9 3.6 %copy-start.1 = (f32[1024,1024]{1,0:T(8,128)S(1)}, f32[1024,1024]{1,0:T(8,128)}, u32[]{:S(2)}) copy-start(f32[1024,1024]{1,0:T(8,128)} %get-tuple-element.163) | copy-start | bytes 12582916 | tf_op jit(solution)/shard_map/while
  216.2 3.6 %copy-start.1 = (f32[1024,1024]{1,0:T(8,128)S(1)}, f32[1024,1024]{1,0:T(8,128)}, u32[]{:S(2)}) copy-start(f32[1024,1024]{1,0:T(8,128)} %get-tuple-element.163) | copy-start | bytes 12582916 | tf_op jit(solution)/shard_map/while
  224.5 3.6 %copy-start.1 = (f32[1024,1024]{1,0:T(8,128)S(1)}, f32[1024,1024]{1,0:T(8,128)}, u32[]{:S(2)}) copy-start(f32[1024,1024]{1,0:T(8,128)} %get-tuple-element.163) | copy-start | bytes 12582916 | tf_op jit(solution)/shard_map/while
  232.8 3.6 %copy-start.1 = (f32[1024,1024]{1,0:T(8,128)S(1)}, f32[1024,1024]{1,0:T(8,128)}, u32[]{:S(2)}) copy-start(f32[1024,1024]{1,0:T(8,128)} %get-tuple-element.163) | copy-start | bytes 12582916 | tf_op jit(solution)/shard_map/while
  257.2 3.4 %copy-start.1 = (f32[1024,1024]{1,0:T(8,128)S(1)}, f32[1024,1024]{1,0:T(8,128)}, u32[]{:S(2)}) copy-start(f32[1024,1024]{1,0:T(8,128)} %get-tuple-element.163) | copy-start | bytes 12582916 | tf_op jit(solution)/shard_map/while
  265.4 3.4 %copy-start.1 = (f32[1024,1024]{1,0:T(8,128)S(1)}, f32[1024,1024]{1,0:T(8,128)}, u32[]{:S(2)}) copy-start(f32[1024,1024]{1,0:T(8,128)} %get-tuple-element.163) | copy-start | bytes 12582916 | tf_op jit(solution)/shard_map/while
  281.6 3.4 %copy-start.1 = (f32[1024,1024]{1,0:T(8,128)S(1)}, f32[1024,1024]{1,0:T(8,128)}, u32[]{:S(2)}) copy-start(f32[1024,1024]{1,0:T(8,128)} %get-tuple-element.163) | copy-start | bytes 12582916 | tf_op jit(solution)/shard_map/while
  289.7 3.4 %copy-start.1 = (f32[1024,1024]{1,0:T(8,128)S(1)}, f32[1024,1024]{1,0:T(8,128)}, u32[]{:S(2)}) copy-start(f32[1024,1024]{1,0:T(8,128)} %get-tuple-element.163) | copy-start | bytes 12582916 | tf_op jit(solution)/shard_map/while
  296.4 16.8 %all-to-all-start.1 = ((bf16[16,2,2048]{2,1,0:T(2,128)(2,1)}), bf16[16,2,2048]{2,1,0:T(2,128)(2,1)S(1)}, u32[]{:S(2)}, u32[]{:S(2)}) async-start(bf16[16,2,2048]{2,1,0:T(2,128)(2,1)} %reshape.590), calls=%async_computation.1 | async-start | bytes 262144 | tf_op jit(solution)/shard_map/all_to_all | solution.py:122
  313.1 16.1 %all-to-all-start.3 = ((bf16[16,9,2,1024]{3,2,1,0:T(2,128)(2,1)}), bf16[16,9,2,1024]{3,2,1,0:T(2,128)(2,1)S(1)}, u32[]{:S(2)}, u32[]{:S(2)}) async-start(bf16[16,9,2,1024]{3,2,1,0:T(2,128)(2,1)} %bitcast.24), calls=%async_computation.4 | async-start | bytes 1179648 | tf_op jit(solution)/shard_map/all_to_all | solution.py:175
  (4 other events, 13.8 us)
Sparse Core Ops, SparseCore 0:
  32.8 72.8 all-gather.4
  108.2 54.3 all-gather.2
  165.2 69.8 reduce-scatter.1
where the time goes:
time: 341 us; the launch traced here: 340 us
  waiting for transfers between devices  101 us (30%)
  matrix products  85.9 us (25%)
  other arithmetic  61.8 us (18%)
  local copies, waits for them, and re-layouts  35 us (10%)
  starting transfers between devices  22.7 us (7%)
  blocking collectives  18.7 us (5%)
  between operations  14.2 us (4%)
    reduce_sum x16, other arithmetic, step_block(): totals = totals * shrink + jnp.sum(raised, axis=-1)  50 us
    dot_general x16, matrix products, step_block(): jnp.einsum('qshd,ksd->qshk', queries, keys_part, preferred_element_type=j...  43.4 us
    all_gather x1, waiting for transfers between devices, mixer_half(): lax.all_gather(key_pairs, 'ep', axis=0, tiled=True)  36.4 us
    all_gather x1, waiting for transfers between devices, expert_half(): lax.all_gather(incoming, 'tp', axis=0, tiled=True)  28.6 us
    all_to_all x1, waiting for transfers between devices, mixer_half(): lax.all_to_all(packed, 'tp', split_axis=2, concat_axis=0, tiled=True)  22.1 us
    all_to_all x1, blocking collectives, expert_half(): lax.all_to_all(outgoing, 'ep', split_axis=0, concat_axis=0, tiled=True)  18.7 us
    squeeze x16, local copies, waits for them, and re-layouts, attend(): return lax.scan(step_block, fold_state, blocks)[0]  15.6 us
    dot_general x16, matrix products, step_block(): jnp.einsum('qshk,ksd->qshd', raised.astype(jnp.bfloat16), values_part, pr...  14.9 us
  transfers between devices with their start and end apart: 6, of which 5 were waited for; matrix products, arithmetic and copies ran while one was open for 49% of the time, Pallas kernels for 0%

commit v1 on v0

--- a/solution.py
+++ b/solution.py
@@ -7,6 +7,13 @@
 HEAD = 64
 GRID_W = 64
 epsilon = 1e-06
+
+
+def gather_over(block, axis, dim):
+    n_dev = lax.axis_size(axis)
+    shards = jnp.stack([block for _ in range(n_dev)])
+    shards = lax.all_to_all(shards, axis, split_axis=0, concat_axis=0)
+    return jnp.concatenate(shards, axis=dim)
 
 
 def normalize(values, gain_vec):
@@ -112,7 +119,7 @@
         jnp.zeros((span_rows, sequences, local_heads, HEAD), jnp.float32),
     )
     running_max, totals, accumulated = attend(
-        own_queries, start_state, lax.all_gather(key_pairs, "ep", axis=0, tiled=True)
+        own_queries, start_state, gather_over(key_pairs, "ep", 0)
     )
     mixed = (
         (accumulated / totals[..., None])

time: 341 us -> 321 us (0.941)
  waiting for transfers between devices: 101 us -> 79 us
    all_gather x1 -> x0, waiting for transfers between devices: 36.4 us -> none  [mixer_half(): lax.all_gather(key_pairs, 'ep', axis=0, tiled=True)]
    all_to_all x0 -> x1, waiting for transfers between devices: none -> 20.4 us  [gather_over(): shards = lax.all_to_all(shards, axis, split_axis=0, concat_axis=0)]
    all_gather x1, waiting for transfers between devices: 28.6 us -> 22.7 us  [expert_half(): lax.all_gather(incoming, 'tp', axis=0, tiled=True)]
    all_to_all x0 -> x1, starting transfers between devices: none -> 4.69 us  [gather_over(): shards = lax.all_to_all(shards, axis, split_axis=0, concat_axis=0)]
    all_to_all x1, starting transfers between devices: 7.87 us -> 4.34 us  [mixer_half(): lax.all_to_all(mixed, 'tp', split_axis=0, concat_axis=2, tiled=True)]
  transfers between devices with their start and end apart: 6 -> 6, of which waited for: 5 -> 5; matrix products, arithmetic and copies ran while one was open for 49% -> 52% of each run, Pallas kernels for 0% -> 0%
where the time goes in v1:
time: 321 us; the launch traced here: 320 us
  matrix products  85.9 us (27%)
  waiting for transfers between devices  79 us (25%)
  other arithmetic  60.8 us (19%)
  local copies, waits for them, and re-layouts  36.5 us (11%)
  starting transfers between devices  23.5 us (7%)
  blocking collectives  18.7 us (6%)
  between operations  14.5 us (5%)
    reduce_sum x16, other arithmetic, step_block(): totals = totals * shrink + jnp.sum(raised, axis=-1)  49.7 us
    dot_general x16, matrix products, step_block(): jnp.einsum('qshd,ksd->qshk', queries, keys_part, preferred_element_type=j...  43.4 us
    all_gather x1, waiting for transfers between devices, expert_half(): lax.all_gather(incoming, 'tp', axis=0, tiled=True)  22.7 us
    all_to_all x1, waiting for transfers between devices, mixer_half(): lax.all_to_all(packed, 'tp', split_axis=2, concat_axis=0, tiled=True)  22.2 us
    all_to_all x1, waiting for transfers between devices, gather_over(): shards = lax.all_to_all(shards, axis, split_axis=0, concat_axis=0)  20.4 us
    all_to_all x1, blocking collectives, expert_half(): lax.all_to_all(outgoing, 'ep', split_axis=0, concat_axis=0, tiled=True)  18.7 us
    squeeze x16, local copies, waits for them, and re-layouts, attend(): return lax.scan(step_block, fold_state, blocks)[0]  15.6 us
    dot_general x16, matrix products, step_block(): jnp.einsum('qshk,ksd->qshd', raised.astype(jnp.bfloat16), values_part, pr...  14.9 us
  transfers between devices with their start and end apart: 6, of which 5 were waited for; matrix products, arithmetic and copies ran while one was open for 52% of the time, Pallas kernels for 0%

profile of v1, /device:TPU:1, one launch (start us, length us, event | category | flops | bytes accessed | tf_op | source)
XLA Modules:
  0.0 319.6 jit_solution(18382692328158582175)
XLA Ops:
  13.0 18.7 %all_to_all.48 = bf16[16,9,2,1024]{3,2,1,0:T(2,128)(2,1)S(1)} all-to-all(bf16[16,9,2,1024]{3,2,1,0:T(2,128)(2,1)S(1)} %reshape.570), channel_id=1, replica_groups=mesh['ep'=16,'tp'=16] {'ep'}, dimensions={0} | all-to-all | bytes 1179648 | tf_op jit(solution)/shard_map/all_to_all | solution.py:174
  37.7 10.4 %all-to-all-start = ((bf16[64,1,16,192]{3,0,1,2:T(8,128)(2,1)}), bf16[64,1,16,192]{3,0,1,2:T(8,128)(2,1)S(1)}, u32[]{:S(2)}, u32[]{:S(2)}) async-start(bf16[64,1,16,192]{3,0,1,2:T(8,128)(2,1)} %pad_maximum_fusion), calls=%async_computation | async-start | bytes 1048576 | tf_op jit(solution)/shard_map/all_to_all | solution.py:104
  48.2 22.2 %all-to-all-done = bf16[64,1,16,192]{3,0,1,2:T(8,128)(2,1)S(1)} async-done(((bf16[64,1,16,192]{3,0,1,2:T(8,128)(2,1)}), bf16[64,1,16,192]{3,0,1,2:T(8,128)(2,1)S(1)}, u32[]{:S(2)}, u32[]{:S(2)}) %all-to-all-start) | async-done | bytes 393248 | tf_op jit(solution)/shard_map/all_to_all | solution.py:104
  77.3 4.7 %all-to-all-start.1 = ((bf16[16,1024,1,128]{3,1,2,0:T(8,128)(2,1)}), bf16[16,1024,1,128]{3,1,2,0:T(8,128)(2,1)}, u32[]{:S(2)}, u32[]{:S(2)}) async-start(bf16[16,1024,1,128]{3,1,2,0:T(8,128)(2,1)} %stack.12), calls=%async_computation.1 | async-start | bytes 8388608 | tf_op jit(solution)/shard_map/all_to_all | solution.py:15
  83.1 22.7 %all-gather.2.cloned.1.call-done = bf16[2304,2,1024]{2,0,1:T(8,128)(2,1)} async-done(((bf16[144,2,1024]{2,0,1:T(8,128)(2,1)}), bf16[2304,2,1024]{2,0,1:T(8,128)(2,1)}) %all-gather.2.cloned.1.call-update) | async-done | bytes 9437200 | tf_op jit(solution)/shard_map/all_gather | solution.py:177
  105.8 8.7 %convolution_bitcast_fusion.1 = f32[2304,2,256]{2,0,1:T(8,128)} fusion(bf16[2304,2,1024]{2,0,1:T(8,128)(2,1)} %all-gather.2.cloned.1.call-done, bf16[2,1024,256]{2,1,0:T(8,128)(2,1)} %param.29), kind=kOutput, calls=%fused_computation.26 | convolution fusion | flops 2415919104 | bytes 15204352 | tf_op jit(solution)/shard_map/rjd,jdf->rjf/dot_general | solution.py:134
  114.5 11.7 %convert_bitcast_fusion = bf16[2304,2,1024]{2,0,1:T(8,128)(2,1)} fusion(bf16[2,256,1024]{2,1,0:T(8,128)(2,1)} %param.31, bf16[2304,2,1024]{2,0,1:T(8,128)(2,1)} %all-gather.2.cloned.1.call-done, bf16[2,1024,256]{2,1,0:T(8,128)(2,1)} %param.30, f32[2304,2,256]{2,0,1:T(8,128)} %convolution_bitcast_fusion.1), kind=kOutput, calls=%fused_computation.23 | convolution fusion | flops 4843634688 | bytes 25690112 | tf_op jit(solution)/shard_map/rjf,jfd->rjd/dot_general | solution.py:140
  126.2 20.4 %all-to-all-done.1 = bf16[16,1024,1,128]{3,1,2,0:T(8,128)(2,1)} async-done(((bf16[16,1024,1,128]{3,1,2,0:T(8,128)(2,1)}), bf16[16,1024,1,128]{3,1,2,0:T(8,128)(2,1)}, u32[]{:S(2)}, u32[]{:S(2)}) %all-to-all-start.1) | async-done | bytes 4194336 | tf_op jit(solution)/shard_map/all_to_all | solution.py:15
  146.7 130.8 %while.15 = (s32[]{:T(128)}, f32[1024,1,1]{0,2,1:T(1,128)S(1)}, f32[1024,1,1]{0,2,1:T(1,128)S(1)}, f32[1024,1,1,64]{0,3,2,1:T(8,128)S(1)}, bf16[16,1024,1,128]{3...) while((s32[]{:T(128)}, f32[1024,1,1]{0,2,1:T(1,128)S(1)}, ...), condition=%wide.region_6.7_spmd.clone, body=%wide.region_3.6_spmd.clone.sunk | while | flops 277025792 | bytes 31129728 | solution.py:81
  150.4 3.2 fusion.81
  158.7 3.2 fusion.81
  167.0 3.2 fusion.81
  175.3 3.2 fusion.81
  183.6 3.2 fusion.81
  191.9 3.2 fusion.81
  200.2 3.1 fusion.81
  208.3 3.1 fusion.81
  216.4 3.1 fusion.81
  224.5 3.1 fusion.81
  240.7 3.1 fusion.81
  279.8 4.3 %all-to-all-start.2 = ((bf16[16,2,2048]{2,1,0:T(2,128)(2,1)}), bf16[16,2,2048]{2,1,0:T(2,128)(2,1)S(1)}, u32[]{:S(2)}, u32[]{:S(2)}) async-start(bf16[16,2,2048]{2,1,0:T(2,128)(2,1)} %reshape.589), calls=%async_computation.2 | async-start | bytes 262144 | tf_op jit(solution)/shard_map/all_to_all | solution.py:129
  287.0 6.0 %all-to-all-done.2 = bf16[16,2,2048]{2,1,0:T(2,128)(2,1)S(1)} async-done(((bf16[16,2,2048]{2,1,0:T(2,128)(2,1)}), bf16[16,2,2048]{2,1,0:T(2,128)(2,1)S(1)}, u32[]{:S(2)}, u32[]{:S(2)}) %all-to-all-start.2) | async-done | bytes 131104 | tf_op jit(solution)/shard_map/all_to_all | solution.py:129
  293.0 3.9 %all-to-all-start.4 = ((bf16[16,9,2,1024]{3,2,1,0:T(2,128)(2,1)}), bf16[16,9,2,1024]{3,2,1,0:T(2,128)(2,1)S(1)}, u32[]{:S(2)}, u32[]{:S(2)}) async-start(bf16[16,9,2,1024]{3,2,1,0:T(2,128)(2,1)} %bitcast.23), calls=%async_computation.5 | async-start | bytes 1179648 | tf_op jit(solution)/shard_map/all_to_all | solution.py:182
  301.1 7.7 %all-to-all-done.4 = bf16[16,9,2,1024]{3,2,1,0:T(2,128)(2,1)S(1)} async-done(((bf16[16,9,2,1024]{3,2,1,0:T(2,128)(2,1)}), bf16[16,9,2,1024]{3,2,1,0:T(2,128)(2,1)S(1)}, u32[]{:S(2)}, u32[]{:S(2)}) %all-to-all-start.4) | async-done | bytes 589856 | tf_op jit(solution)/shard_map/all_to_all | solution.py:182
  (227 shorter events, 128.8 us)
Async XLA Ops:
  7.2 28.7 %copy-start = (bf16[1024,1024]{1,0:T(8,128)(2,1)S(1)}, bf16[1024,1024]{1,0:T(8,128)(2,1)}, u32[]{:S(2)}) copy-start(bf16[1024,1024]{1,0:T(8,128)(2,1)} %param.19) | copy-start | bytes 6291460
  7.2 25.5 %copy-start.2 = (bf16[64,1,1024]{2,0,1:T(8,128)(2,1)S(1)}, bf16[64,1,1024]{2,0,1:T(8,128)(2,1)}, u32[]{:S(2)}) copy-start(bf16[64,1,1024]{2,0,1:T(8,128)(2,1)} %param.17) | copy-start | bytes 393220
  7.2 25.7 %copy-start.4 = (f32[1024]{0:T(1024)S(1)}, f32[1024]{0:T(1024)}, u32[]{:S(2)}) copy-start(f32[1024]{0:T(1024)} %param.18) | copy-start | bytes 12292
  7.2 98.6 %all-gather.2.cloned.1.call-start = ((), (), s32[]{:S(2)}) async-start(), calls=%async_computation.6 | async-start | bytes 10027008 | tf_op jit(solution)/shard_map/all_gather | solution.py:177
  32.7 15.4 %copy-start.7 = (f32[64]{0:T(128)S(1)}, f32[64]{0:T(128)}, u32[]{:S(2)}) copy-start(f32[64]{0:T(128)} %param.23) | copy-start | bytes 772
  37.7 32.7 %all-to-all-start = ((bf16[64,1,16,192]{3,0,1,2:T(8,128)(2,1)}), bf16[64,1,16,192]{3,0,1,2:T(8,128)(2,1)S(1)}, u32[]{:S(2)}, u32[]{:S(2)}) async-start(bf16[64,1,16,192]{3,0,1,2:T(8,128)(2,1)} %pad_maximum_fusion), calls=%async_computation | async-start | bytes 1048576 | tf_op jit(solution)/shard_map/all_to_all | solution.py:104
  77.3 5.0 %copy-start.3 = (bf16[1024,1,1,64]{3,0,2,1:T(8,128)(2,1)S(1)}, bf16[1024,1,1,64]{3,0,2,1:T(8,128)(2,1)}, u32[]{:S(2)}) copy-start(bf16[1024,1,1,64]{3,0,2,1:T(8,128)(2,1)} %get-tuple-element.76) | copy-start | bytes 393220
  77.3 5.2 %copy-start.6 = (f32[64]{0:T(128)S(1)}, f32[64]{0:T(128)}, u32[]{:S(2)}) copy-start(f32[64]{0:T(128)} %param.22) | copy-start | bytes 772
  77.3 69.4 %all-to-all-start.1 = ((bf16[16,1024,1,128]{3,1,2,0:T(8,128)(2,1)}), bf16[16,1024,1,128]{3,1,2,0:T(8,128)(2,1)}, u32[]{:S(2)}, u32[]{:S(2)}) async-start(bf16[16,1024,1,128]{3,1,2,0:T(8,128)(2,1)} %stack.12), calls=%async_computation.1 | async-start | bytes 8388608 | tf_op jit(solution)/shard_map/all_to_all | solution.py:15
  82.0 202.6 %reduce-scatter.2.cloned.1.call-start = ((), (), s32[]{:S(2)}) async-start(), calls=%async_computation.7 | async-start | bytes 10027008 | tf_op jit(solution)/shard_map/reduce_scatter | solution.py:178
  146.7 137.7 %copy-start.5 = (f32[128,2]{0,1:T(2,128)S(1)}, f32[128,2]{0,1:T(2,128)}, u32[]{:S(2)}) copy-start(f32[128,2]{0,1:T(2,128)} %param.28) | copy-start | bytes 3076
  150.4 3.6 %copy-start.1 = (f32[1024,1024]{1,0:T(8,128)S(1)}, f32[1024,1024]{1,0:T(8,128)}, u32[]{:S(2)}) copy-start(f32[1024,1024]{1,0:T(8,128)} %get-tuple-element.127) | copy-start | bytes 12582916 | tf_op jit(solution)/shard_map/while
  158.7 3.6 %copy-start.1 = (f32[1024,1024]{1,0:T(8,128)S(1)}, f32[1024,1024]{1,0:T(8,128)}, u32[]{:S(2)}) copy-start(f32[1024,1024]{1,0:T(8,128)} %get-tuple-element.127) | copy-start | bytes 12582916 | tf_op jit(solution)/shard_map/while
  167.0 3.6 %copy-start.1 = (f32[1024,1024]{1,0:T(8,128)S(1)}, f32[1024,1024]{1,0:T(8,128)}, u32[]{:S(2)}) copy-start(f32[1024,1024]{1,0:T(8,128)} %get-tuple-element.127) | copy-start | bytes 12582916 | tf_op jit(solution)/shard_map/while
  175.3 3.6 %copy-start.1 = (f32[1024,1024]{1,0:T(8,128)S(1)}, f32[1024,1024]{1,0:T(8,128)}, u32[]{:S(2)}) copy-start(f32[1024,1024]{1,0:T(8,128)} %get-tuple-element.127) | copy-start | bytes 12582916 | tf_op jit(solution)/shard_map/while
  183.6 3.6 %copy-start.1 = (f32[1024,1024]{1,0:T(8,128)S(1)}, f32[1024,1024]{1,0:T(8,128)}, u32[]{:S(2)}) copy-start(f32[1024,1024]{1,0:T(8,128)} %get-tuple-element.127) | copy-start | bytes 12582916 | tf_op jit(solution)/shard_map/while
  191.9 3.6 %copy-start.1 = (f32[1024,1024]{1,0:T(8,128)S(1)}, f32[1024,1024]{1,0:T(8,128)}, u32[]{:S(2)}) copy-start(f32[1024,1024]{1,0:T(8,128)} %get-tuple-element.127) | copy-start | bytes 12582916 | tf_op jit(solution)/shard_map/while
  200.1 3.4 %copy-start.1 = (f32[1024,1024]{1,0:T(8,128)S(1)}, f32[1024,1024]{1,0:T(8,128)}, u32[]{:S(2)}) copy-start(f32[1024,1024]{1,0:T(8,128)} %get-tuple-element.127) | copy-start | bytes 12582916 | tf_op jit(solution)/shard_map/while
  208.2 3.4 %copy-start.1 = (f32[1024,1024]{1,0:T(8,128)S(1)}, f32[1024,1024]{1,0:T(8,128)}, u32[]{:S(2)}) copy-start(f32[1024,1024]{1,0:T(8,128)} %get-tuple-element.127) | copy-start | bytes 12582916 | tf_op jit(solution)/shard_map/while
  232.6 3.4 %copy-start.1 = (f32[1024,1024]{1,0:T(8,128)S(1)}, f32[1024,1024]{1,0:T(8,128)}, u32[]{:S(2)}) copy-start(f32[1024,1024]{1,0:T(8,128)} %get-tuple-element.127) | copy-start | bytes 12582916 | tf_op jit(solution)/shard_map/while
  256.9 3.4 %copy-start.1 = (f32[1024,1024]{1,0:T(8,128)S(1)}, f32[1024,1024]{1,0:T(8,128)}, u32[]{:S(2)}) copy-start(f32[1024,1024]{1,0:T(8,128)} %get-tuple-element.127) | copy-start | bytes 12582916 | tf_op jit(solution)/shard_map/while
  273.1 3.4 %copy-start.1 = (f32[1024,1024]{1,0:T(8,128)S(1)}, f32[1024,1024]{1,0:T(8,128)}, u32[]{:S(2)}) copy-start(f32[1024,1024]{1,0:T(8,128)} %get-tuple-element.127) | copy-start | bytes 12582916 | tf_op jit(solution)/shard_map/while
  279.8 13.2 %all-to-all-start.2 = ((bf16[16,2,2048]{2,1,0:T(2,128)(2,1)}), bf16[16,2,2048]{2,1,0:T(2,128)(2,1)S(1)}, u32[]{:S(2)}, u32[]{:S(2)}) async-start(bf16[16,2,2048]{2,1,0:T(2,128)(2,1)} %reshape.589), calls=%async_computation.2 | async-start | bytes 262144 | tf_op jit(solution)/shard_map/all_to_all | solution.py:129
  293.0 15.7 %all-to-all-start.4 = ((bf16[16,9,2,1024]{3,2,1,0:T(2,128)(2,1)}), bf16[16,9,2,1024]{3,2,1,0:T(2,128)(2,1)S(1)}, u32[]{:S(2)}, u32[]{:S(2)}) async-start(bf16[16,9,2,1024]{3,2,1,0:T(2,128)(2,1)} %bitcast.23), calls=%async_computation.5 | async-start | bytes 1179648 | tf_op jit(solution)/shard_map/all_to_all | solution.py:182
  (5 other events, 17.2 us)
Sparse Core Ops, SparseCore 0:
  32.8 72.8 all-gather.1
  126.4 68.2 reduce-scatter.1
